TPU v7x, 32 devices: a whole 2x2x4 slice. The times are simulated.
32 devices in a mesh: fs: 8 (over z, y), tp: 4 (over x, core).
Axes of the slice: x: 2, y: 2, z: 4, core: 2. Of those that a mesh axis runs over, the one named last changes fastest.
Arguments:
- tokens: bfloat16 [3072, 2048], P(('fs', 'tp')), may hold values from -6 to 6
- ffn1_gain: float32 [2048], replicated, may hold values from 0.1 to 1.9
- ffn1_gate: bfloat16 [2048, 5632], P('fs', 'tp'), may hold values from -0.125 to 0.125
- ffn1_up: bfloat16 [2048, 5632], P('fs', 'tp'), may hold values from -0.125 to 0.125
- ffn1_down: bfloat16 [5632, 2048], P('tp', 'fs'), may hold values from -0.078125 to 0.078125
- mix_gain: float32 [2048], replicated, may hold values from 0.1 to 1.9
- lru_in_weight: bfloat16 [2048, 1536], P('fs', 'tp'), may hold values from -0.125 to 0.125
- lru_gate_weight: bfloat16 [2048, 1536], P('fs', 'tp'), may hold values from -0.125 to 0.125
- conv_weight: bfloat16 [4, 1536], P(None, 'tp'), may hold values from -3 to 3
- gate_a_weight: bfloat16 [24, 64, 64], P('tp'), may hold values from -0.75 to 0.75
- gate_x_weight: bfloat16 [24, 64, 64], P('tp'), may hold values from -0.75 to 0.75
- decay_param: float32 [1536], P('tp'), may hold values from 3.7 to 9
- mix_out_weight: bfloat16 [1536, 2048], P('tp', 'fs'), may hold values from -0.15625 to 0.15625
- ffn2_gain: float32 [2048], replicated, may hold values from 0.1 to 1.9
- ffn2_gate: bfloat16 [2048, 5632], P('fs', 'tp'), may hold values from -0.125 to 0.125
- ffn2_up: bfloat16 [2048, 5632], P('fs', 'tp'), may hold values from -0.125 to 0.125
- ffn2_down: bfloat16 [5632, 2048], P('tp', 'fs'), may hold values from -0.078125 to 0.078125
Outputs:
- layer_out: bfloat16 [3072, 2048], P(('fs', 'tp'))
All inputs are finite; a program needn't handle non-finite values.
Results may differ from a plain program's by a relative error of at most 0.017.
Values may be sent and summed in bfloat16 or wider, within the bound.
A program may use at most 64 MiB of HBM per device.

v0:
```python
import math

import jax
import jax.numpy as jnp
from jax import lax
from jax.experimental import pallas as pl
from jax.sharding import PartitionSpec as P

EPS = 1e-06
CORES = 2
SHARE_FIRST = 4
SHARE_MIX = 2
SHARE_SECOND = 4


def rms_rows(values, gain):
    wide = values.astype(jnp.float32)
    scale = lax.rsqrt(jnp.mean(wide * wide, axis=-1, keepdims=True) + EPS)
    return (wide * scale * gain).astype(jnp.bfloat16)


def pick(stack, index):
    return lax.dynamic_index_in_dim(stack, index, 0, keepdims=False)


def share_weights(blocks, n):
    shares, high, wide = blocks.shape
    me = lax.axis_index("fs")
    chosen = [pick(blocks, (me + j) % shares) for j in range(shares)]
    whole = jnp.zeros((high, n * wide), blocks.dtype)
    for d in range(n):
        piece = chosen[d % shares]
        if d:
            piece = lax.ppermute(piece, "fs", [(i, (i + d) % n) for i in range(n)])
        whole = lax.dynamic_update_slice(whole, piece, (0, ((me - d) % n) * wide))
    return whole


def steps_of(shares, xs):
    return [(j, k) for j in range(shares) for k in range(xs)]


def route(n, t, shares, j, k):
    xs = t // CORES
    pairs = []
    for f in range(n):
        for x in range(xs):
            for c in range(CORES):
                to_f = f // shares * shares + (f % shares + j) % shares
                to_t = (x + k) % xs * CORES + c
                pairs.append((f * t + x * CORES + c, to_f * t + to_t))
    return pairs


def swap_core(values, t):
    return lax.ppermute(values, "tp", [(i, i ^ 1) for i in range(t)])


def send(values, pairs):
    return lax.ppermute(values, ("fs", "tp"), pairs)


def gather_cell(rows, n, t, shares):
    got = [
        send(rows, route(n, t, shares, j, k)) if j or k else rows
        for j, k in steps_of(shares, t // CORES)
    ]
    own = jnp.concatenate(got, axis=0)
    return own, swap_core(own, t)


def scatter_cell(own, other, local, n, t, shares):
    xs = t // CORES
    both = own + swap_core(other.astype(jnp.bfloat16), t).astype(jnp.float32)
    low = both.astype(jnp.bfloat16)
    total = both[:local]
    for s, (j, k) in enumerate(steps_of(shares, xs)):
        if s:
            back = [(b, a) for a, b in route(n, t, shares, j, k)]
            part = send(low[s * local : (s + 1) * local], back)
            total = total + part.astype(jnp.float32)
    return total


def dot_nt(a, b):
    return lax.dot_general(a, b, (((1,), (1,)), ((), ())), preferred_element_type=jnp.float32)


def in_pair(first, second, shares, n):
    stack = jnp.concatenate(
        [w.T.reshape(shares, -1, w.shape[0]) for w in (first, second)], axis=1
    )
    return share_weights(stack, n)


def out_share(weight, shares, n):
    return share_weights(weight.reshape(shares, -1, weight.shape[1]), n)


def half_block(normed, pair, down, n, t, shares):
    half = pair.shape[0] // 2

    def terms(rows):
        both = dot_nt(rows, pair)
        hidden = (jax.nn.silu(both[:, :half]) * both[:, half:]).astype(jnp.bfloat16)
        return jnp.dot(hidden, down, preferred_element_type=jnp.float32)

    own, other = gather_cell(normed, n, t, shares)
    other_terms = terms(other)
    return scatter_cell(terms(own), other_terms, normed.shape[0], n, t, shares)


def scan_kernel(keep_ref, drive_ref, out_ref):
    keep, state = keep_ref[0], drive_ref[0]
    length = keep.shape[0]
    step = 1
    while step < length:
        ones = jnp.ones((step, keep.shape[1]), jnp.float32)
        zeros = jnp.zeros((step, keep.shape[1]), jnp.float32)
        state = state + keep * jnp.concatenate([zeros, state[: length - step]], axis=0)
        keep = keep * jnp.concatenate([ones, keep[: length - step]], axis=0)
        step *= 2
    out_ref[0] = state


def scan_rows(keep, drive):
    seqs, length, channels = keep.shape
    spec = pl.BlockSpec((1, length, channels), lambda i: (i, 0, 0))
    return pl.pallas_call(
        scan_kernel,
        grid=(seqs,),
        in_specs=[spec, spec],
        out_specs=spec,
        out_shape=jax.ShapeDtypeStruct(keep.shape, jnp.float32),
        cost_estimate=pl.CostEstimate(
            flops=30 * keep.size, bytes_accessed=12 * keep.size, transcendentals=0
        ),
    )(keep, drive)


def mixer(normed, pair, out, conv_weight, gate_a_weight, gate_x_weight, decay_param, n, t, shares):
    local = normed.shape[0]
    xs = t // CORES
    place = lax.axis_index("fs") % shares
    tp = lax.axis_index("tp")
    x, core = tp // CORES, tp % CORES
    steps = steps_of(shares, xs)
    own, other = gather_cell(normed, n, t, shares)
    low = jnp.concatenate([dot_nt(own, pair), dot_nt(other, pair)], axis=0).astype(jnp.bfloat16)
    width = low.shape[1]
    low = low.reshape(2 * len(steps), local, width)
    ordered = []
    for s in range(shares):
        for a in range(xs):
            at = ((place - s) % shares) * xs + (x - a) % xs
            for c in range(CORES):
                ordered.append(pick(low, at + jnp.where(core == c, 0, len(steps))))
    channels = width // 2
    both = jnp.concatenate(ordered, axis=0).reshape(shares, t * local, width).astype(jnp.float32)
    lru_low, gate_low = both[..., :channels], both[..., channels:]
    blocks_here = gate_a_weight.shape[0] // shares
    gate_a = lax.dynamic_slice_in_dim(gate_a_weight, place * blocks_here, blocks_here, 0)
    gate_x = lax.dynamic_slice_in_dim(gate_x_weight, place * blocks_here, blocks_here, 0)
    taps = lax.dynamic_slice_in_dim(conv_weight, place * channels, channels, 1).astype(jnp.float32)
    decay = lax.dynamic_slice_in_dim(decay_param, place * channels, channels, 0)
    length = t * local
    count = taps.shape[0]
    padded = jnp.pad(lru_low, ((0, 0), (count - 1, 0), (0, 0)))
    conv = jnp.zeros_like(lru_low)
    for offset in range(count):
        conv = conv + taps[offset] * padded[:, count - 1 - offset : count - 1 - offset + length]
    conv_low = conv.astype(jnp.bfloat16)
    eye = jnp.eye(blocks_here, dtype=jnp.bfloat16)
    flat = conv_low.reshape(shares * length, channels)

    def gate(weight):
        dense = (eye[:, None, :, None] * weight[:, :, None, :]).reshape(channels, channels)
        return jax.nn.sigmoid(
            jnp.dot(flat, dense, preferred_element_type=jnp.float32)
        ).reshape(shares, length, channels)

    recall, admit = gate(gate_a), gate(gate_x)
    log_keep = -8.0 * recall * jax.nn.softplus(-decay)
    drive = jnp.sqrt(-jnp.expm1(2.0 * log_keep)) * admit * conv_low.astype(jnp.float32)
    state = scan_rows(jnp.exp(log_keep), drive)
    mixed = (state * jax.nn.gelu(gate_low)).astype(jnp.bfloat16)
    mixed = mixed.reshape(shares * t, local, channels)
    sides = []
    for side in (core, 1 - core):
        rows = [
            pick(mixed, ((place - j) % shares) * t + ((x - k) % xs) * CORES + side)
            for j, k in steps
        ]
        sides.append(
            jnp.dot(jnp.concatenate(rows, axis=0), out, preferred_element_type=jnp.float32)
        )
    return scatter_cell(sides[0], sides[1], local, n, t, shares)


def body(
    n,
    t,
    tokens,
    ffn1_gain,
    ffn1_gate,
    ffn1_up,
    ffn1_down,
    mix_gain,
    lru_in_weight,
    lru_gate_weight,
    conv_weight,
    gate_a_weight,
    gate_x_weight,
    decay_param,
    mix_out_weight,
    ffn2_gain,
    ffn2_gate,
    ffn2_up,
    ffn2_down,
):
    share_mix = math.gcd(SHARE_MIX, gate_a_weight.shape[0], n)
    pair1 = in_pair(ffn1_gate, ffn1_up, SHARE_FIRST, n)
    down1 = out_share(ffn1_down, SHARE_FIRST, n)
    pair_mix = in_pair(lru_in_weight, lru_gate_weight, share_mix, n)
    out_mix = out_share(mix_out_weight, share_mix, n)
    pair2 = in_pair(ffn2_gate, ffn2_up, SHARE_SECOND, n)
    down2 = out_share(ffn2_down, SHARE_SECOND, n)
    sums = half_block(rms_rows(tokens, ffn1_gain), pair1, down1, n, t, SHARE_FIRST)
    first = (tokens.astype(jnp.float32) + 0.5 * sums).astype(jnp.bfloat16)
    sums = mixer(
        rms_rows(first, mix_gain),
        pair_mix,
        out_mix,
        conv_weight,
        gate_a_weight,
        gate_x_weight,
        decay_param,
        n,
        t,
        share_mix,
    )
    second = (first.astype(jnp.float32) + sums).astype(jnp.bfloat16)
    sums = half_block(rms_rows(second, ffn2_gain), pair2, down2, n, t, SHARE_SECOND)
    return (second.astype(jnp.float32) + 0.5 * sums).astype(jnp.bfloat16)


def solution(mesh):
    n, t = mesh.shape["fs"], mesh.shape["tp"]
    in_specs = (
        P(("fs", "tp"), None),
        P(),
        P("fs", "tp"),
        P("fs", "tp"),
        P("tp", "fs"),
        P(),
        P("fs", "tp"),
        P("fs", "tp"),
        P(None, "tp"),
        P("tp", None, None),
        P("tp", None, None),
        P("tp"),
        P("tp", "fs"),
        P(),
        P("fs", "tp"),
        P("fs", "tp"),
        P("tp", "fs"),
    )
    out_specs = P(("fs", "tp"), None)

    def run(*args):
        return body(n, t, *args)

    return jax.shard_map(run, mesh=mesh, in_specs=in_specs, out_specs=out_specs, check_vma=False)
```

profile of v0, /device:TPU:0, one launch (start us, length us, event | category | flops | bytes accessed | tf_op | source)
XLA Modules:
  0.0 544.6 jit_solution(3988439728923266106)
XLA Ops:
  22.6 10.5 %collective-permute-done.2 = bf16[96,2048]{1,0:T(8,128)(2,1)S(1)} collective-permute-done((bf16[96,2048]{1,0:T(8,128)(2,1)S(1)}, bf16[96,2048]{1,0:T(8,128)(2,1)S(1)}, u32[]{:S(2)}, u32[]{:S(2)}) %collective-permute-start.2) | collective-permute-done | bytes 393248 | tf_op jit(solution)/shard_map/ppermute | solution.py:60
  35.5 7.5 %collective-permute-done.5 = bf16[96,2048]{1,0:T(8,128)(2,1)S(1)} collective-permute-done((bf16[96,2048]{1,0:T(8,128)(2,1)S(1)}, bf16[96,2048]{1,0:T(8,128)(2,1)S(1)}, u32[]{:S(2)}, u32[]{:S(2)}) %collective-permute-start.5) | collective-permute-done | bytes 393248 | tf_op jit(solution)/shard_map/ppermute | solution.py:60
  64.1 8.9 %collective-permute-start.17 = (bf16[352,256]{1,0:T(8,128)(2,1)S(1)}, bf16[352,256]{1,0:T(8,128)(2,1)S(1)}, u32[]{:S(2)}, u32[]{:S(2)}) collective-permute-start(bf16[352,256]{1,0:T(8,128)(2,1)S(1)} %get-tuple-element.24), channel_id=1, source_target_pairs={{0,16},{4,20},{8,24},{12,28},{16,0},{20,4},{24,8},{28,12},{1,17},{... | collective-permute-start | bytes 540680 | tf_op jit(solution)/shard_map/ppermute | solution.py:34
  73.9 8.5 %collective-permute-done.16 = bf16[352,256]{1,0:T(8,128)(2,1)S(1)} collective-permute-done((bf16[352,256]{1,0:T(8,128)(2,1)S(1)}, bf16[352,256]{1,0:T(8,128)(2,1)S(1)}, u32[]{:S(2)}, u32[]{:S(2)}) %collective-permute-start.16) | collective-permute-done | bytes 180256 | tf_op jit(solution)/shard_map/ppermute | solution.py:34
  89.1 7.7 %collective-permute-done.20 = bf16[352,256]{1,0:T(8,128)(2,1)S(1)} collective-permute-done((bf16[352,256]{1,0:T(8,128)(2,1)S(1)}, bf16[352,256]{1,0:T(8,128)(2,1)S(1)}, u32[]{:S(2)}, u32[]{:S(2)}) %collective-permute-start.20) | collective-permute-done | bytes 180256 | tf_op jit(solution)/shard_map/ppermute | solution.py:34
  101.6 17.3 %collective-permute-done.9 = bf16[704,256]{1,0:T(8,128)(2,1)S(1)} collective-permute-done((bf16[704,256]{1,0:T(8,128)(2,1)S(1)}, bf16[704,256]{1,0:T(8,128)(2,1)S(1)}, u32[]{:S(2)}, u32[]{:S(2)}) %collective-permute-start.9) | collective-permute-done | bytes 360480 | tf_op jit(solution)/shard_map/ppermute | solution.py:34
  120.3 17.3 %collective-permute-done.10 = bf16[704,256]{1,0:T(8,128)(2,1)S(1)} collective-permute-done((bf16[704,256]{1,0:T(8,128)(2,1)S(1)}, bf16[704,256]{1,0:T(8,128)(2,1)S(1)}, u32[]{:S(2)}, u32[]{:S(2)}) %collective-permute-start.10) | collective-permute-done | bytes 360480 | tf_op jit(solution)/shard_map/ppermute | solution.py:34
  154.6 5.3 fusion.112
  166.7 14.4 %collective-permute-start.24 = (bf16[96,2048]{1,0:T(8,128)(2,1)S(1)}, bf16[96,2048]{1,0:T(8,128)(2,1)S(1)}, u32[]{:S(2)}, u32[]{:S(2)}) collective-permute-start(bf16[96,2048]{1,0:T(8,128)(2,1)S(1)} %get-tuple-element.38), channel_id=1, source_target_pairs={{4,0},{5,1},{6,2},{7,3},{8,4},{9,5},{10,6},{11,7},{12,8},{13,9},{1... | collective-permute-start | bytes 1179656 | tf_op jit(solution)/shard_map/ppermute | solution.py:60
  193.6 5.6 %collective-permute-done.25 = bf16[96,2048]{1,0:T(8,128)(2,1)S(1)} collective-permute-done((bf16[96,2048]{1,0:T(8,128)(2,1)}, bf16[96,2048]{1,0:T(8,128)(2,1)S(1)}, u32[]{:S(2)}, u32[]{:S(2)}) %collective-permute-start.25) | collective-permute-done | bytes 393248 | tf_op jit(solution)/shard_map/ppermute | solution.py:60
  199.6 8.0 %collective-permute-done.26 = bf16[96,2048]{1,0:T(8,128)(2,1)S(1)} collective-permute-done((bf16[96,2048]{1,0:T(8,128)(2,1)}, bf16[96,2048]{1,0:T(8,128)(2,1)S(1)}, u32[]{:S(2)}, u32[]{:S(2)}) %collective-permute-start.26) | collective-permute-done | bytes 393248 | tf_op jit(solution)/shard_map/ppermute | solution.py:60
  209.7 6.3 %collective-permute-done.27 = bf16[96,2048]{1,0:T(8,128)(2,1)S(1)} collective-permute-done((bf16[96,2048]{1,0:T(8,128)(2,1)}, bf16[96,2048]{1,0:T(8,128)(2,1)S(1)}, u32[]{:S(2)}, u32[]{:S(2)}) %collective-permute-start.27) | collective-permute-done | bytes 393248 | tf_op jit(solution)/shard_map/ppermute | solution.py:60
  216.0 8.4 %collective-permute-done.29 = bf16[96,2048]{1,0:T(8,128)(2,1)S(1)} collective-permute-done((bf16[96,2048]{1,0:T(8,128)(2,1)}, bf16[96,2048]{1,0:T(8,128)(2,1)S(1)}, u32[]{:S(2)}, u32[]{:S(2)}) %collective-permute-start.29) | collective-permute-done | bytes 393248 | tf_op jit(solution)/shard_map/ppermute | solution.py:60
  245.4 5.9 %collective-permute-done.31 = bf16[96,2048]{1,0:T(8,128)(2,1)} collective-permute-done((bf16[96,2048]{1,0:T(8,128)(2,1)S(1)}, bf16[96,2048]{1,0:T(8,128)(2,1)}, u32[]{:S(2)}, u32[]{:S(2)}) %collective-permute-start.31) | collective-permute-done | bytes 393248 | tf_op jit(solution)/shard_map/ppermute | solution.py:60
  267.3 5.3 collective-permute-done.34
  274.5 10.1 %collective-permute-done.36 = bf16[384,256]{1,0:T(8,128)(2,1)S(1)} collective-permute-done((bf16[384,256]{1,0:T(8,128)(2,1)S(1)}, bf16[384,256]{1,0:T(8,128)(2,1)S(1)}, u32[]{:S(2)}, u32[]{:S(2)}) %collective-permute-start.36) | collective-permute-done | bytes 196640 | tf_op jit(solution)/shard_map/ppermute | solution.py:34
  312.6 5.3 collective-permute-start.50
  318.5 5.3 collective-permute-done.49
  323.7 11.0 %collective-permute-done.50 = bf16[96,2048]{1,0:T(8,128)(2,1)S(1)} collective-permute-done((bf16[96,2048]{1,0:T(8,128)(2,1)S(1)}, bf16[96,2048]{1,0:T(8,128)(2,1)S(1)}, u32[]{:S(2)}, u32[]{:S(2)}) %collective-permute-start.50) | collective-permute-done | bytes 393248 | tf_op jit(solution)/shard_map/ppermute | solution.py:60
  339.7 7.7 %collective-permute-start.54 = (bf16[96,2048]{1,0:T(8,128)(2,1)S(1)}, bf16[96,2048]{1,0:T(8,128)(2,1)S(1)}, u32[]{:S(2)}, u32[]{:S(2)}) collective-permute-start(bf16[96,2048]{1,0:T(8,128)(2,1)S(1)} %get-tuple-element.8), channel_id=1, source_target_pairs={{0,6},{1,7},{2,4},{3,5},{4,10},{5,11},{6,8},{7,9},{8,14},{9,15},{1... | collective-permute-start | bytes 1179656 | tf_op jit(solution)/shard_map/ppermute | solution.py:60
  349.7 5.5 %collective-permute-start.57 = (bf16[96,2048]{1,0:T(8,128)(2,1)S(1)}, bf16[96,2048]{1,0:T(8,128)(2,1)S(1)}, u32[]{:S(2)}, u32[]{:S(2)}) collective-permute-start(bf16[96,2048]{1,0:T(8,128)(2,1)S(1)} %get-tuple-element.8), channel_id=1, source_target_pairs={{0,12},{1,13},{2,14},{3,15},{4,0},{5,1},{6,2},{7,3},{8,4},{9,5},{1... | collective-permute-start | bytes 1179656 | tf_op jit(solution)/shard_map/ppermute | solution.py:60
  368.9 10.6 %collective-permute-done.57 = bf16[96,2048]{1,0:T(8,128)(2,1)S(1)} collective-permute-done((bf16[96,2048]{1,0:T(8,128)(2,1)S(1)}, bf16[96,2048]{1,0:T(8,128)(2,1)S(1)}, u32[]{:S(2)}, u32[]{:S(2)}) %collective-permute-start.57) | collective-permute-done | bytes 393248 | tf_op jit(solution)/shard_map/ppermute | solution.py:60
  400.7 6.2 %collective-permute-start.69 = (bf16[352,256]{1,0:T(8,128)(2,1)S(1)}, bf16[352,256]{1,0:T(8,128)(2,1)S(1)}, u32[]{:S(2)}, u32[]{:S(2)}) collective-permute-start(bf16[352,256]{1,0:T(8,128)(2,1)S(1)} %get-tuple-element.12), channel_id=1, source_target_pairs={{0,16},{4,20},{8,24},{12,28},{16,0},{20,4},{24,8},{28,12},{1,17},{... | collective-permute-start | bytes 540680 | tf_op jit(solution)/shard_map/ppermute | solution.py:34
  407.8 9.8 %collective-permute-done.68 = bf16[352,256]{1,0:T(8,128)(2,1)S(1)} collective-permute-done((bf16[352,256]{1,0:T(8,128)(2,1)S(1)}, bf16[352,256]{1,0:T(8,128)(2,1)S(1)}, u32[]{:S(2)}, u32[]{:S(2)}) %collective-permute-start.68) | collective-permute-done | bytes 180256 | tf_op jit(solution)/shard_map/ppermute | solution.py:34
  427.9 5.8 %collective-permute-done.59 = bf16[704,256]{1,0:T(8,128)(2,1)S(1)} collective-permute-done((bf16[704,256]{1,0:T(8,128)(2,1)S(1)}, bf16[704,256]{1,0:T(8,128)(2,1)S(1)}, u32[]{:S(2)}, u32[]{:S(2)}) %collective-permute-start.59) | collective-permute-done | bytes 360480 | tf_op jit(solution)/shard_map/ppermute | solution.py:34
  433.8 7.2 %collective-permute-start.62 = (bf16[704,256]{1,0:T(8,128)(2,1)S(1)}, bf16[704,256]{1,0:T(8,128)(2,1)S(1)}, u32[]{:S(2)}, u32[]{:S(2)}) collective-permute-start(bf16[704,256]{1,0:T(8,128)(2,1)S(1)} %get-tuple-element.6), channel_id=1, source_target_pairs={{0,16},{4,20},{8,24},{12,28},{16,0},{20,4},{24,8},{28,12},{1,17},{... | collective-permute-start | bytes 1081352 | tf_op jit(solution)/shard_map/ppermute | solution.py:34
  441.1 15.8 %collective-permute-done.61 = bf16[704,256]{1,0:T(8,128)(2,1)S(1)} collective-permute-done((bf16[704,256]{1,0:T(8,128)(2,1)S(1)}, bf16[704,256]{1,0:T(8,128)(2,1)S(1)}, u32[]{:S(2)}, u32[]{:S(2)}) %collective-permute-start.61) | collective-permute-done | bytes 360480 | tf_op jit(solution)/shard_map/ppermute | solution.py:34
  457.2 15.5 %collective-permute-done.62 = bf16[704,256]{1,0:T(8,128)(2,1)S(1)} collective-permute-done((bf16[704,256]{1,0:T(8,128)(2,1)S(1)}, bf16[704,256]{1,0:T(8,128)(2,1)S(1)}, u32[]{:S(2)}, u32[]{:S(2)}) %collective-permute-start.62) | collective-permute-done | bytes 360480 | tf_op jit(solution)/shard_map/ppermute | solution.py:34
  488.5 16.6 %collective-permute-start.76 = (bf16[96,2048]{1,0:T(8,128)(2,1)S(1)}, bf16[96,2048]{1,0:T(8,128)(2,1)S(1)}, u32[]{:S(2)}, u32[]{:S(2)}) collective-permute-start(bf16[96,2048]{1,0:T(8,128)(2,1)S(1)} %get-tuple-element.31), channel_id=1, source_target_pairs={{4,0},{5,1},{6,2},{7,3},{8,4},{9,5},{10,6},{11,7},{12,8},{13,9},{1... | collective-permute-start | bytes 1179656 | tf_op jit(solution)/shard_map/ppermute | solution.py:60
  514.6 8.5 %collective-permute-done.77 = bf16[96,2048]{1,0:T(8,128)(2,1)S(1)} collective-permute-done((bf16[96,2048]{1,0:T(8,128)(2,1)S(1)}, bf16[96,2048]{1,0:T(8,128)(2,1)S(1)}, u32[]{:S(2)}, u32[]{:S(2)}) %collective-permute-start.77) | collective-permute-done | bytes 393248 | tf_op jit(solution)/shard_map/ppermute | solution.py:60
  523.1 8.4 %collective-permute-done.78 = bf16[96,2048]{1,0:T(8,128)(2,1)S(1)} collective-permute-done((bf16[96,2048]{1,0:T(8,128)(2,1)S(1)}, bf16[96,2048]{1,0:T(8,128)(2,1)S(1)}, u32[]{:S(2)}, u32[]{:S(2)}) %collective-permute-start.78) | collective-permute-done | bytes 393248 | tf_op jit(solution)/shard_map/ppermute | solution.py:60
  531.5 7.3 %collective-permute-done.79 = bf16[96,2048]{1,0:T(8,128)(2,1)S(1)} collective-permute-done((bf16[96,2048]{1,0:T(8,128)(2,1)S(1)}, bf16[96,2048]{1,0:T(8,128)(2,1)S(1)}, u32[]{:S(2)}, u32[]{:S(2)}) %collective-permute-start.79) | collective-permute-done | bytes 393248 | tf_op jit(solution)/shard_map/ppermute | solution.py:60
  (312 shorter events, 249.8 us)
Async XLA Ops:
  9.2 25.5 %collective-permute-start.4 = (bf16[96,2048]{1,0:T(8,128)(2,1)S(1)}, bf16[96,2048]{1,0:T(8,128)(2,1)S(1)}, u32[]{:S(2)}, u32[]{:S(2)}) collective-permute-start(bf16[96,2048]{1,0:T(8,128)(2,1)S(1)} %get-tuple-element.22), channel_id=1, source_target_pairs={{0,10},{1,11},{2,8},{3,9},{4,14},{5,15},{6,12},{7,13},{8,2},{9,3},... | collective-permute-start | bytes 1179656 | tf_op jit(solution)/shard_map/ppermute | solution.py:60
  16.1 26.9 %collective-permute-start.5 = (bf16[96,2048]{1,0:T(8,128)(2,1)S(1)}, bf16[96,2048]{1,0:T(8,128)(2,1)S(1)}, u32[]{:S(2)}, u32[]{:S(2)}) collective-permute-start(bf16[96,2048]{1,0:T(8,128)(2,1)S(1)} %get-tuple-element.22), channel_id=1, source_target_pairs={{0,12},{1,13},{2,14},{3,15},{4,0},{5,1},{6,2},{7,3},{8,4},{9,5},{1... | collective-permute-start | bytes 1179656 | tf_op jit(solution)/shard_map/ppermute | solution.py:60
  19.9 26.5 %collective-permute-start.6 = (bf16[96,2048]{1,0:T(8,128)(2,1)S(1)}, bf16[96,2048]{1,0:T(8,128)(2,1)S(1)}, u32[]{:S(2)}, u32[]{:S(2)}) collective-permute-start(bf16[96,2048]{1,0:T(8,128)(2,1)S(1)} %get-tuple-element.22), channel_id=1, source_target_pairs={{0,14},{1,15},{2,12},{3,13},{4,2},{5,3},{6,0},{7,1},{8,6},{9,7},{1... | collective-permute-start | bytes 1179656 | tf_op jit(solution)/shard_map/ppermute | solution.py:60
  47.2 93.6 %collective-permute-start.21 = (bf16[768,2048]{1,0:T(8,128)(2,1)}, bf16[768,2048]{1,0:T(8,128)(2,1)}, u32[]{:S(2)}, u32[]{:S(2)}) collective-permute-start(bf16[768,2048]{1,0:T(8,128)(2,1)} %constant_dynamic-update-slice_fusion), channel_id=1, source_target_pairs={{0,1},{1,0},{2,3},{3,2},{4,5},{5,4},{6,7},{7,6},{8,9},{9,8},{10,11... | collective-permute-start | bytes 9437192 | tf_op jit(solution)/shard_map/ppermute | solution.py:56
  51.1 35.7 %collective-permute-start.18 = (bf16[352,256]{1,0:T(8,128)(2,1)}, bf16[352,256]{1,0:T(8,128)(2,1)}, u32[]{:S(2)}, u32[]{:S(2)}) collective-permute-start(bf16[352,256]{1,0:T(8,128)(2,1)} %get-tuple-element.55), channel_id=1, source_target_pairs={{0,20},{4,24},{8,28},{12,0},{16,4},{20,8},{24,12},{28,16},{1,21},{... | collective-permute-start | bytes 540680 | tf_op jit(solution)/shard_map/ppermute | solution.py:34
  54.4 33.5 %collective-permute-start.19 = (bf16[352,256]{1,0:T(8,128)(2,1)}, bf16[352,256]{1,0:T(8,128)(2,1)}, u32[]{:S(2)}, u32[]{:S(2)}) collective-permute-start(bf16[352,256]{1,0:T(8,128)(2,1)} %get-tuple-element.54), channel_id=1, source_target_pairs={{0,24},{4,28},{8,0},{12,4},{16,8},{20,12},{24,16},{28,20},{1,25},{... | collective-permute-start | bytes 540680 | tf_op jit(solution)/shard_map/ppermute | solution.py:34
  87.9 31.1 %collective-permute-start.9 = (bf16[704,256]{1,0:T(8,128)(2,1)S(1)}, bf16[704,256]{1,0:T(8,128)(2,1)S(1)}, u32[]{:S(2)}, u32[]{:S(2)}) collective-permute-start(bf16[704,256]{1,0:T(8,128)(2,1)S(1)} %get-tuple-element.45), channel_id=1, source_target_pairs={{0,12},{4,16},{8,20},{12,24},{16,28},{20,0},{24,4},{28,8},{1,13},{... | collective-permute-start | bytes 1081352 | tf_op jit(solution)/shard_map/ppermute | solution.py:34
  96.8 41.5 %collective-permute-start.11 = (bf16[704,256]{1,0:T(8,128)(2,1)S(1)}, bf16[704,256]{1,0:T(8,128)(2,1)S(1)}, u32[]{:S(2)}, u32[]{:S(2)}) collective-permute-start(bf16[704,256]{1,0:T(8,128)(2,1)S(1)} %get-tuple-element.46), channel_id=1, source_target_pairs={{0,20},{4,24},{8,28},{12,0},{16,4},{20,8},{24,12},{28,16},{1,21},{... | collective-permute-start | bytes 1081352 | tf_op jit(solution)/shard_map/ppermute | solution.py:34
  96.9 40.7 %collective-permute-start.10 = (bf16[704,256]{1,0:T(8,128)(2,1)S(1)}, bf16[704,256]{1,0:T(8,128)(2,1)S(1)}, u32[]{:S(2)}, u32[]{:S(2)}) collective-permute-start(bf16[704,256]{1,0:T(8,128)(2,1)S(1)} %copy-done.12), channel_id=1, source_target_pairs={{0,16},{4,20},{8,24},{12,28},{16,0},{20,4},{24,8},{28,12},{1,17},{... | collective-permute-start | bytes 1081352 | tf_op jit(solution)/shard_map/ppermute | solution.py:34
  100.1 39.1 %collective-permute-start.12 = (bf16[704,256]{1,0:T(8,128)(2,1)S(1)}, bf16[704,256]{1,0:T(8,128)(2,1)S(1)}, u32[]{:S(2)}, u32[]{:S(2)}) collective-permute-start(bf16[704,256]{1,0:T(8,128)(2,1)S(1)} %get-tuple-element.47), channel_id=1, source_target_pairs={{0,24},{4,28},{8,0},{12,4},{16,8},{20,12},{24,16},{28,20},{1,25},{... | collective-permute-start | bytes 1081352 | tf_op jit(solution)/shard_map/ppermute | solution.py:34
  182.4 33.6 %collective-permute-start.27 = (bf16[96,2048]{1,0:T(8,128)(2,1)}, bf16[96,2048]{1,0:T(8,128)(2,1)S(1)}, u32[]{:S(2)}, u32[]{:S(2)}) collective-permute-start(bf16[96,2048]{1,0:T(8,128)(2,1)} %get-tuple-element.35), channel_id=1, source_target_pairs={{10,0},{11,1},{8,2},{9,3},{14,4},{15,5},{12,6},{13,7},{2,8},{3,9},... | collective-permute-start | bytes 1179656 | tf_op jit(solution)/shard_map/ppermute | solution.py:60
  184.8 31.2 %collective-permute-start.28 = (bf16[96,2048]{1,0:T(8,128)(2,1)}, bf16[96,2048]{1,0:T(8,128)(2,1)S(1)}, u32[]{:S(2)}, u32[]{:S(2)}) collective-permute-start(bf16[96,2048]{1,0:T(8,128)(2,1)} %get-tuple-element.34), channel_id=1, source_target_pairs={{12,0},{13,1},{14,2},{15,3},{0,4},{1,5},{2,6},{3,7},{4,8},{5,9},{6... | collective-permute-start | bytes 1179656 | tf_op jit(solution)/shard_map/ppermute | solution.py:60
  190.5 33.9 %collective-permute-start.29 = (bf16[96,2048]{1,0:T(8,128)(2,1)}, bf16[96,2048]{1,0:T(8,128)(2,1)S(1)}, u32[]{:S(2)}, u32[]{:S(2)}) collective-permute-start(bf16[96,2048]{1,0:T(8,128)(2,1)} %get-tuple-element.33), channel_id=1, source_target_pairs={{14,0},{15,1},{12,2},{13,3},{2,4},{3,5},{0,6},{1,7},{6,8},{7,9},{4... | collective-permute-start | bytes 1179656 | tf_op jit(solution)/shard_map/ppermute | solution.py:60
  199.2 33.2 %collective-permute-start.41 = (bf16[192,256]{1,0:T(8,128)(2,1)}, bf16[192,256]{1,0:T(8,128)(2,1)}, u32[]{:S(2)}, u32[]{:S(2)}) collective-permute-start(bf16[192,256]{1,0:T(8,128)(2,1)} %dynamic-slice_bitcast_fusion.8), channel_id=1, source_target_pairs={{0,4},{4,8},{8,12},{12,16},{16,20},{20,24},{24,28},{28,0},{1,5},{5... | collective-permute-start | bytes 294920 | tf_op jit(solution)/shard_map/ppermute | solution.py:34
  207.6 31.5 %collective-permute-start.43 = (bf16[192,256]{1,0:T(8,128)(2,1)}, bf16[192,256]{1,0:T(8,128)(2,1)}, u32[]{:S(2)}, u32[]{:S(2)}) collective-permute-start(bf16[192,256]{1,0:T(8,128)(2,1)} %dynamic-slice_bitcast_fusion.8), channel_id=1, source_target_pairs={{0,12},{4,16},{8,20},{12,24},{16,28},{20,0},{24,4},{28,8},{1,13},{... | collective-permute-start | bytes 294920 | tf_op jit(solution)/shard_map/ppermute | solution.py:34
  239.0 27.1 %collective-permute-start.33 = (bf16[384,256]{1,0:T(8,128)(2,1)}, bf16[384,256]{1,0:T(8,128)(2,1)S(1)}, u32[]{:S(2)}, u32[]{:S(2)}) collective-permute-start(bf16[384,256]{1,0:T(8,128)(2,1)} %fusion.72), channel_id=1, source_target_pairs={{0,4},{4,8},{8,12},{12,16},{16,20},{20,24},{24,28},{28,0},{1,5},{5... | collective-permute-start | bytes 589832 | tf_op jit(solution)/shard_map/ppermute | solution.py:34
  239.1 35.3 %collective-permute-start.35 = (bf16[384,256]{1,0:T(8,128)(2,1)}, bf16[384,256]{1,0:T(8,128)(2,1)S(1)}, u32[]{:S(2)}, u32[]{:S(2)}) collective-permute-start(bf16[384,256]{1,0:T(8,128)(2,1)} %fusion.72), channel_id=1, source_target_pairs={{0,12},{4,16},{8,20},{12,24},{16,28},{20,0},{24,4},{28,8},{1,13},{... | collective-permute-start | bytes 589832 | tf_op jit(solution)/shard_map/ppermute | solution.py:34
  257.0 32.0 %collective-permute-start.40 = (bf16[384,2048]{1,0:T(8,128)(2,1)S(1)}, bf16[384,2048]{1,0:T(8,128)(2,1)S(1)}, u32[]{:S(2)}, u32[]{:S(2)}) collective-permute-start(bf16[384,2048]{1,0:T(8,128)(2,1)S(1)} %pad_maximum_fusion), channel_id=1, source_target_pairs={{0,1},{1,0},{2,3},{3,2},{4,5},{5,4},{6,7},{7,6},{8,9},{9,8},{10,11... | collective-permute-start | bytes 4718600 | tf_op jit(solution)/shard_map/ppermute | solution.py:56
  349.7 29.8 %collective-permute-start.57 = (bf16[96,2048]{1,0:T(8,128)(2,1)S(1)}, bf16[96,2048]{1,0:T(8,128)(2,1)S(1)}, u32[]{:S(2)}, u32[]{:S(2)}) collective-permute-start(bf16[96,2048]{1,0:T(8,128)(2,1)S(1)} %get-tuple-element.8), channel_id=1, source_target_pairs={{0,12},{1,13},{2,14},{3,15},{4,0},{5,1},{6,2},{7,3},{8,4},{9,5},{1... | collective-permute-start | bytes 1179656 | tf_op jit(solution)/shard_map/ppermute | solution.py:60
  356.3 26.6 %collective-permute-start.58 = (bf16[96,2048]{1,0:T(8,128)(2,1)S(1)}, bf16[96,2048]{1,0:T(8,128)(2,1)S(1)}, u32[]{:S(2)}, u32[]{:S(2)}) collective-permute-start(bf16[96,2048]{1,0:T(8,128)(2,1)S(1)} %get-tuple-element.8), channel_id=1, source_target_pairs={{0,14},{1,15},{2,12},{3,13},{4,2},{5,3},{6,0},{7,1},{8,6},{9,7},{1... | collective-permute-start | bytes 1179656 | tf_op jit(solution)/shard_map/ppermute | solution.py:60
  383.6 89.3 %collective-permute-start.73 = (bf16[768,2048]{1,0:T(8,128)(2,1)}, bf16[768,2048]{1,0:T(8,128)(2,1)}, u32[]{:S(2)}, u32[]{:S(2)}) collective-permute-start(bf16[768,2048]{1,0:T(8,128)(2,1)} %constant_dynamic-update-slice_fusion.8), channel_id=1, source_target_pairs={{0,1},{1,0},{2,3},{3,2},{4,5},{5,4},{6,7},{7,6},{8,9},{9,8},{10,11... | collective-permute-start | bytes 9437192 | tf_op jit(solution)/shard_map/ppermute | solution.py:56
  385.5 36.5 %collective-permute-start.70 = (bf16[352,256]{1,0:T(8,128)(2,1)}, bf16[352,256]{1,0:T(8,128)(2,1)}, u32[]{:S(2)}, u32[]{:S(2)}) collective-permute-start(bf16[352,256]{1,0:T(8,128)(2,1)} %get-tuple-element.52), channel_id=1, source_target_pairs={{0,20},{4,24},{8,28},{12,0},{16,4},{20,8},{24,12},{28,16},{1,21},{... | collective-permute-start | bytes 540680 | tf_op jit(solution)/shard_map/ppermute | solution.py:34
  389.7 33.3 %collective-permute-start.71 = (bf16[352,256]{1,0:T(8,128)(2,1)}, bf16[352,256]{1,0:T(8,128)(2,1)}, u32[]{:S(2)}, u32[]{:S(2)}) collective-permute-start(bf16[352,256]{1,0:T(8,128)(2,1)} %get-tuple-element.51), channel_id=1, source_target_pairs={{0,24},{4,28},{8,0},{12,4},{16,8},{20,12},{24,16},{28,20},{1,25},{... | collective-permute-start | bytes 540680 | tf_op jit(solution)/shard_map/ppermute | solution.py:34
  423.0 33.9 %collective-permute-start.61 = (bf16[704,256]{1,0:T(8,128)(2,1)S(1)}, bf16[704,256]{1,0:T(8,128)(2,1)S(1)}, u32[]{:S(2)}, u32[]{:S(2)}) collective-permute-start(bf16[704,256]{1,0:T(8,128)(2,1)S(1)} %get-tuple-element.42), channel_id=1, source_target_pairs={{0,12},{4,16},{8,20},{12,24},{16,28},{20,0},{24,4},{28,8},{1,13},{... | collective-permute-start | bytes 1081352 | tf_op jit(solution)/shard_map/ppermute | solution.py:34
  424.7 48.0 %collective-permute-start.63 = (bf16[704,256]{1,0:T(8,128)(2,1)S(1)}, bf16[704,256]{1,0:T(8,128)(2,1)S(1)}, u32[]{:S(2)}, u32[]{:S(2)}) collective-permute-start(bf16[704,256]{1,0:T(8,128)(2,1)S(1)} %get-tuple-element.43), channel_id=1, source_target_pairs={{0,20},{4,24},{8,28},{12,0},{16,4},{20,8},{24,12},{28,16},{1,21},{... | collective-permute-start | bytes 1081352 | tf_op jit(solution)/shard_map/ppermute | solution.py:34
  433.8 38.9 %collective-permute-start.62 = (bf16[704,256]{1,0:T(8,128)(2,1)S(1)}, bf16[704,256]{1,0:T(8,128)(2,1)S(1)}, u32[]{:S(2)}, u32[]{:S(2)}) collective-permute-start(bf16[704,256]{1,0:T(8,128)(2,1)S(1)} %get-tuple-element.6), channel_id=1, source_target_pairs={{0,16},{4,20},{8,24},{12,28},{16,0},{20,4},{24,8},{28,12},{1,17},{... | collective-permute-start | bytes 1081352 | tf_op jit(solution)/shard_map/ppermute | solution.py:34
  441.0 31.8 %collective-permute-start.64 = (bf16[704,256]{1,0:T(8,128)(2,1)S(1)}, bf16[704,256]{1,0:T(8,128)(2,1)S(1)}, u32[]{:S(2)}, u32[]{:S(2)}) collective-permute-start(bf16[704,256]{1,0:T(8,128)(2,1)S(1)} %get-tuple-element.44), channel_id=1, source_target_pairs={{0,24},{4,28},{8,0},{12,4},{16,8},{20,12},{24,16},{28,20},{1,25},{... | collective-permute-start | bytes 1081352 | tf_op jit(solution)/shard_map/ppermute | solution.py:34
  488.5 26.1 %collective-permute-start.76 = (bf16[96,2048]{1,0:T(8,128)(2,1)S(1)}, bf16[96,2048]{1,0:T(8,128)(2,1)S(1)}, u32[]{:S(2)}, u32[]{:S(2)}) collective-permute-start(bf16[96,2048]{1,0:T(8,128)(2,1)S(1)} %get-tuple-element.31), channel_id=1, source_target_pairs={{4,0},{5,1},{6,2},{7,3},{8,4},{9,5},{10,6},{11,7},{12,8},{13,9},{1... | collective-permute-start | bytes 1179656 | tf_op jit(solution)/shard_map/ppermute | solution.py:60
  505.3 26.2 %collective-permute-start.78 = (bf16[96,2048]{1,0:T(8,128)(2,1)S(1)}, bf16[96,2048]{1,0:T(8,128)(2,1)S(1)}, u32[]{:S(2)}, u32[]{:S(2)}) collective-permute-start(bf16[96,2048]{1,0:T(8,128)(2,1)S(1)} %get-tuple-element.29), channel_id=1, source_target_pairs={{8,0},{9,1},{10,2},{11,3},{12,4},{13,5},{14,6},{15,7},{0,8},{1,9},... | collective-permute-start | bytes 1179656 | tf_op jit(solution)/shard_map/ppermute | solution.py:60
  505.3 33.5 %collective-permute-start.79 = (bf16[96,2048]{1,0:T(8,128)(2,1)S(1)}, bf16[96,2048]{1,0:T(8,128)(2,1)S(1)}, u32[]{:S(2)}, u32[]{:S(2)}) collective-permute-start(bf16[96,2048]{1,0:T(8,128)(2,1)S(1)} %get-tuple-element.28), channel_id=1, source_target_pairs={{10,0},{11,1},{8,2},{9,3},{14,4},{15,5},{12,6},{13,7},{2,8},{3,9},... | collective-permute-start | bytes 1179656 | tf_op jit(solution)/shard_map/ppermute | solution.py:60
  508.0 30.8 %collective-permute-start.80 = (bf16[96,2048]{1,0:T(8,128)(2,1)S(1)}, bf16[96,2048]{1,0:T(8,128)(2,1)S(1)}, u32[]{:S(2)}, u32[]{:S(2)}) collective-permute-start(bf16[96,2048]{1,0:T(8,128)(2,1)S(1)} %get-tuple-element.27), channel_id=1, source_target_pairs={{12,0},{13,1},{14,2},{15,3},{0,4},{1,5},{2,6},{3,7},{4,8},{5,9},{6... | collective-permute-start | bytes 1179656 | tf_op jit(solution)/shard_map/ppermute | solution.py:60
  514.6 28.5 %collective-permute-start.81 = (bf16[96,2048]{1,0:T(8,128)(2,1)S(1)}, bf16[96,2048]{1,0:T(8,128)(2,1)S(1)}, u32[]{:S(2)}, u32[]{:S(2)}) collective-permute-start(bf16[96,2048]{1,0:T(8,128)(2,1)S(1)} %get-tuple-element.26), channel_id=1, source_target_pairs={{14,0},{15,1},{12,2},{13,3},{2,4},{3,5},{0,6},{1,7},{6,8},{7,9},{4... | collective-permute-start | bytes 1179656 | tf_op jit(solution)/shard_map/ppermute | solution.py:60
  (73 other events, 1319.2 us)
where the time goes:
time: 551 us; the launch traced here: 545 us
  waiting for transfers between devices  264 us (48%)
  starting transfers between devices  173 us (31%)
  local copies, waits for them, and re-layouts  45.8 us (8%)
  matrix products  38.8 us (7%)
  other arithmetic  19 us (3%)
    ppermute x34, waiting for transfers between devices, send(): return lax.ppermute(values, ('fs', 'tp'), pairs)  133 us
    ppermute x42, waiting for transfers between devices, share_weights(): piece = lax.ppermute(piece, 'fs', [(i, (i + d) % n) for i in range(n)])  126 us
    ppermute x34, starting transfers between devices, send(): return lax.ppermute(values, ('fs', 'tp'), pairs)  89.2 us
    ppermute x42, starting transfers between devices, share_weights(): piece = lax.ppermute(piece, 'fs', [(i, (i + d) % n) for i in range(n)])  83.4 us
    dot_general x6, matrix products, dot_nt(): lax.dot_general(a, b, (((1,), (1,)), ((), ())), preferred_element_type=jn...  22.6 us
    dynamic_update_slice x45, local copies, waits for them, and re-layouts, share_weights(): whole = lax.dynamic_update_slice(whole, piece, (0, (me - d) % n * wide))  16.4 us
    unnamed x71, local copies, waits for them, and re-layouts  12.4 us
    dot_general x4, matrix products, terms(): return jnp.dot(hidden, down, preferred_element_type=jnp.float32)  11.8 us
  transfers between devices with their start and end apart: 82, of which 43 were waited for; matrix products, arithmetic and copies ran while one was open for 10% of the time, Pallas kernels for 0%

commit v1 on v0

--- a/solution.py
+++ b/solution.py
@@ -23,15 +23,26 @@
     return lax.dynamic_index_in_dim(stack, index, 0, keepdims=False)
 
 
-def share_weights(blocks, n):
-    shares, high, wide = blocks.shape
+def send_shares(blocks, n):
+    shares = blocks.shape[0]
     me = lax.axis_index("fs")
-    chosen = [pick(blocks, (me + j) % shares) for j in range(shares)]
-    whole = jnp.zeros((high, n * wide), blocks.dtype)
+    pieces = []
     for d in range(n):
-        piece = chosen[d % shares]
+        piece = pick(blocks, (me + d) % shares)
         if d:
             piece = lax.ppermute(piece, "fs", [(i, (i + d) % n) for i in range(n)])
+        pieces.append(piece)
+    return pieces
+
+
+def assemble(pieces, tie=None):
+    n = len(pieces)
+    high, wide = pieces[0].shape
+    me = lax.axis_index("fs")
+    whole = jnp.zeros((high, n * wide), pieces[0].dtype)
+    for d, piece in enumerate(pieces):
+        if d and tie is not None:
+            piece, _ = lax.optimization_barrier((piece, tie))
         whole = lax.dynamic_update_slice(whole, piece, (0, ((me - d) % n) * wide))
     return whole
 
@@ -60,52 +71,51 @@
     return lax.ppermute(values, ("fs", "tp"), pairs)
 
 
-def gather_cell(rows, n, t, shares):
+def gather_own(rows, n, t, shares):
     got = [
         send(rows, route(n, t, shares, j, k)) if j or k else rows
         for j, k in steps_of(shares, t // CORES)
     ]
-    own = jnp.concatenate(got, axis=0)
-    return own, swap_core(own, t)
+    return jnp.concatenate(got, axis=0), got[1]
 
 
 def scatter_cell(own, other, local, n, t, shares):
     xs = t // CORES
     both = own + swap_core(other.astype(jnp.bfloat16), t).astype(jnp.float32)
     low = both.astype(jnp.bfloat16)
-    total = both[:local]
+    total, early = both[:local], None
     for s, (j, k) in enumerate(steps_of(shares, xs)):
         if s:
             back = [(b, a) for a, b in route(n, t, shares, j, k)]
             part = send(low[s * local : (s + 1) * local], back)
+            early = part if early is None else early
             total = total + part.astype(jnp.float32)
-    return total
+    return total, early
 
 
 def dot_nt(a, b):
     return lax.dot_general(a, b, (((1,), (1,)), ((), ())), preferred_element_type=jnp.float32)
 
 
-def in_pair(first, second, shares, n):
+def gather_shares(first, second, out, shares, n):
     stack = jnp.concatenate(
-        [w.T.reshape(shares, -1, w.shape[0]) for w in (first, second)], axis=1
+        [w.reshape(shares, -1, w.shape[1]) for w in (first.T, second.T, out)], axis=1
     )
-    return share_weights(stack, n)
-
-
-def out_share(weight, shares, n):
-    return share_weights(weight.reshape(shares, -1, weight.shape[1]), n)
-
-
-def half_block(normed, pair, down, n, t, shares):
-    half = pair.shape[0] // 2
+    return send_shares(stack, n)
+
+
+def half_block(normed, pieces, n, t, shares, late):
+    own, early = gather_own(normed, n, t, shares)
+    other = swap_core(own, t)
+    weights = assemble(pieces, early if late else None)
+    part = weights.shape[0] // 3
+    own, weights = lax.optimization_barrier((own, weights))
 
     def terms(rows):
-        both = dot_nt(rows, pair)
-        hidden = (jax.nn.silu(both[:, :half]) * both[:, half:]).astype(jnp.bfloat16)
-        return jnp.dot(hidden, down, preferred_element_type=jnp.float32)
-
-    own, other = gather_cell(normed, n, t, shares)
+        both = dot_nt(rows, weights[: 2 * part])
+        hidden = (jax.nn.silu(both[:, :part]) * both[:, part:]).astype(jnp.bfloat16)
+        return jnp.dot(hidden, weights[2 * part :], preferred_element_type=jnp.float32)
+
     other_terms = terms(other)
     return scatter_cell(terms(own), other_terms, normed.shape[0], n, t, shares)
 
@@ -138,14 +148,17 @@
     )(keep, drive)
 
 
-def mixer(normed, pair, out, conv_weight, gate_a_weight, gate_x_weight, decay_param, n, t, shares):
+def mixer(normed, weights, conv_weight, gate_a_weight, gate_x_weight, decay_param, n, t, shares):
     local = normed.shape[0]
     xs = t // CORES
     place = lax.axis_index("fs") % shares
     tp = lax.axis_index("tp")
     x, core = tp // CORES, tp % CORES
     steps = steps_of(shares, xs)
-    own, other = gather_cell(normed, n, t, shares)
+    part = weights.shape[0] // 3
+    pair, out = weights[: 2 * part], weights[2 * part :]
+    own, _ = gather_own(normed, n, t, shares)
+    other = swap_core(own, t)
     low = jnp.concatenate([dot_nt(own, pair), dot_nt(other, pair)], axis=0).astype(jnp.bfloat16)
     width = low.shape[1]
     low = low.reshape(2 * len(steps), local, width)
@@ -219,18 +232,15 @@
     ffn2_down,
 ):
     share_mix = math.gcd(SHARE_MIX, gate_a_weight.shape[0], n)
-    pair1 = in_pair(ffn1_gate, ffn1_up, SHARE_FIRST, n)
-    down1 = out_share(ffn1_down, SHARE_FIRST, n)
-    pair_mix = in_pair(lru_in_weight, lru_gate_weight, share_mix, n)
-    out_mix = out_share(mix_out_weight, share_mix, n)
-    pair2 = in_pair(ffn2_gate, ffn2_up, SHARE_SECOND, n)
-    down2 = out_share(ffn2_down, SHARE_SECOND, n)
-    sums = half_block(rms_rows(tokens, ffn1_gain), pair1, down1, n, t, SHARE_FIRST)
+    pieces1 = gather_shares(ffn1_gate, ffn1_up, ffn1_down, SHARE_FIRST, n)
+    pieces_mix = gather_shares(lru_in_weight, lru_gate_weight, mix_out_weight, share_mix, n)
+    pieces2 = gather_shares(ffn2_gate, ffn2_up, ffn2_down, SHARE_SECOND, n)
+    sums, early = half_block(rms_rows(tokens, ffn1_gain), pieces1, n, t, SHARE_FIRST, False)
+    sums, weights_mix = lax.optimization_barrier((sums, assemble(pieces_mix, early)))
     first = (tokens.astype(jnp.float32) + 0.5 * sums).astype(jnp.bfloat16)
-    sums = mixer(
+    sums, _ = mixer(
         rms_rows(first, mix_gain),
-        pair_mix,
-        out_mix,
+        weights_mix,
         conv_weight,
         gate_a_weight,
         gate_x_weight,
@@ -240,7 +250,7 @@
         share_mix,
     )
     second = (first.astype(jnp.float32) + sums).astype(jnp.bfloat16)
-    sums = half_block(rms_rows(second, ffn2_gain), pair2, down2, n, t, SHARE_SECOND)
+    sums, _ = half_block(rms_rows(second, ffn2_gain), pieces2, n, t, SHARE_SECOND, True)
     return (second.astype(jnp.float32) + 0.5 * sums).astype(jnp.bfloat16)
 
 

time: 551 us -> 542 us (0.984)
  starting transfers between devices: 173 us -> 158 us
  waiting for transfers between devices: 264 us -> 278 us
    ppermute x34, starting transfers between devices: 89.2 us -> 71.2 us  [send(): return lax.ppermute(values, ('fs', 'tp'), pairs)]
    ppermute x34, waiting for transfers between devices: 133 us -> 140 us  [send(): return lax.ppermute(values, ('fs', 'tp'), pairs)]
    ppermute x42 -> x21, waiting for transfers between devices: 126 us -> 132 us  [send_shares(): piece = lax.ppermute(piece, 'fs', [(i, (i + d) % n) for i in range(n)])]
    ppermute x42 -> x21, starting transfers between devices: 83.4 us -> 86.4 us  [send_shares(): piece = lax.ppermute(piece, 'fs', [(i, (i + d) % n) for i in range(n)])]
    unnamed x71 -> x81, local copies, waits for them, and re-layouts: 12.4 us -> 9.99 us
    dynamic_update_slice x45 -> x24, local copies, waits for them, and re-layouts: 16.4 us -> 15 us  [assemble(): whole = lax.dynamic_update_slice(whole, piece, (0, (me - d) % n * wide))]
  transfers between devices with their start and end apart: 82 -> 61, of which waited for: 43 -> 33; matrix products, arithmetic and copies ran while one was open for 10% -> 10% of each run, Pallas kernels for 0% -> 0%
where the time goes in v1:
time: 542 us; the launch traced here: 539 us
  waiting for transfers between devices  278 us (51%)
  starting transfers between devices  158 us (29%)
  local copies, waits for them, and re-layouts  40.5 us (7%)
  matrix products  40 us (7%)
  other arithmetic  18.5 us (3%)
    ppermute x34, waiting for transfers between devices, send(): return lax.ppermute(values, ('fs', 'tp'), pairs)  140 us
    ppermute x21, waiting for transfers between devices, send_shares(): piece = lax.ppermute(piece, 'fs', [(i, (i + d) % n) for i in range(n)])  132 us
    ppermute x21, starting transfers between devices, send_shares(): piece = lax.ppermute(piece, 'fs', [(i, (i + d) % n) for i in range(n)])  86.4 us
    ppermute x34, starting transfers between devices, send(): return lax.ppermute(values, ('fs', 'tp'), pairs)  71.2 us
    dot_general x6, matrix products, dot_nt(): lax.dot_general(a, b, (((1,), (1,)), ((), ())), preferred_element_type=jn...  19.9 us
    dot_general x4, matrix products, terms(): jnp.dot(hidden, weights[2 * part:], preferred_element_type=jnp.float32)  15.5 us
    dynamic_update_slice x24, local copies, waits for them, and re-layouts, assemble(): whole = lax.dynamic_update_slice(whole, piece, (0, (me - d) % n * wide))  15 us
  transfers between devices with their start and end apart: 61, of which 33 were waited for; matrix products, arithmetic and copies ran while one was open for 10% of the time, Pallas kernels for 0%

profile of v1, /device:TPU:0, one launch (start us, length us, event | category | flops | bytes accessed | tf_op | source)
XLA Modules:
  0.0 539.4 jit_solution(10984926173420865185)
XLA Ops:
  22.6 10.5 %collective-permute-done.2 = bf16[96,2048]{1,0:T(8,128)(2,1)S(1)} collective-permute-done((bf16[96,2048]{1,0:T(8,128)(2,1)S(1)}, bf16[96,2048]{1,0:T(8,128)(2,1)S(1)}, u32[]{:S(2)}, u32[]{:S(2)}) %collective-permute-start.2) | collective-permute-done | bytes 393248 | tf_op jit(solution)/shard_map/ppermute | solution.py:71
  35.4 7.5 %collective-permute-done.5 = bf16[96,2048]{1,0:T(8,128)(2,1)S(1)} collective-permute-done((bf16[96,2048]{1,0:T(8,128)(2,1)S(1)}, bf16[96,2048]{1,0:T(8,128)(2,1)S(1)}, u32[]{:S(2)}, u32[]{:S(2)}) %collective-permute-start.5) | collective-permute-done | bytes 393248 | tf_op jit(solution)/shard_map/ppermute | solution.py:71
  62.3 8.9 %collective-permute-done.7 = bf16[1056,256]{1,0:T(8,128)(2,1)} collective-permute-done((bf16[1056,256]{1,0:T(8,128)(2,1)}, bf16[1056,256]{1,0:T(8,128)(2,1)}, u32[]{:S(2)}, u32[]{:S(2)}) %collective-permute-start.7) | collective-permute-done | bytes 540704 | tf_op jit(solution)/shard_map/ppermute | solution.py:33
  77.1 40.3 %collective-permute-done.9 = bf16[1056,256]{1,0:T(8,128)(2,1)} collective-permute-done((bf16[1056,256]{1,0:T(8,128)(2,1)}, bf16[1056,256]{1,0:T(8,128)(2,1)}, u32[]{:S(2)}, u32[]{:S(2)}) %collective-permute-start.9) | collective-permute-done | bytes 540704 | tf_op jit(solution)/shard_map/ppermute | solution.py:33
  117.4 14.7 %collective-permute-start.13 = (bf16[1056,256]{1,0:T(8,128)(2,1)S(1)}, bf16[1056,256]{1,0:T(8,128)(2,1)S(1)}, u32[]{:S(2)}, u32[]{:S(2)}) collective-permute-start(bf16[1056,256]{1,0:T(8,128)(2,1)S(1)} %get-tuple-element.74), channel_id=1, source_target_pairs={{0,28},{4,0},{8,4},{12,8},{16,12},{20,16},{24,20},{28,24},{1,29},{... | collective-permute-start | bytes 1622024 | tf_op jit(solution)/shard_map/ppermute | solution.py:33
  139.9 5.2 fusion.4
  151.7 5.2 fusion.6
  157.0 6.8 %fusion.118 = (bf16[768,2048]{1,0:T(8,128)(2,1)S(1)}, f32[768,2048]{1,0:T(8,128)}) fusion(bf16[768,2048]{1,0:T(8,128)(2,1)} %collective-permute-done.15, bf16[1056,2048]{1,0:T(8,128)(2,1)} %constant_dynamic-update-slice_fusion.30, f32[768,704]{0,1:T(8,128)S(1)} %fusion.6), kind=kOutput, calls=%fused_computation.220 | convolution fusion | flops 1113636864 | bytes 16187392 | tf_op jit(solution)/shard_map/dot_general | solution.py:117
  166.4 15.2 %collective-permute-start.24 = (bf16[576,256]{1,0:T(8,128)(2,1)}, bf16[576,256]{1,0:T(8,128)(2,1)}, u32[]{:S(2)}, u32[]{:S(2)}) collective-permute-start(bf16[576,256]{1,0:T(8,128)(2,1)} %get-tuple-element.91), channel_id=1, source_target_pairs={{0,8},{4,12},{8,16},{12,20},{16,24},{20,28},{24,0},{28,4},{1,9},{5... | collective-permute-start | bytes 884744 | tf_op jit(solution)/shard_map/ppermute | solution.py:33
  188.1 6.2 %collective-permute-start.27 = (bf16[576,256]{1,0:T(8,128)(2,1)}, bf16[576,256]{1,0:T(8,128)(2,1)S(1)}, u32[]{:S(2)}, u32[]{:S(2)}) collective-permute-start(bf16[576,256]{1,0:T(8,128)(2,1)} %get-tuple-element.88), channel_id=1, source_target_pairs={{0,20},{4,24},{8,28},{12,0},{16,4},{20,8},{24,12},{28,16},{1,21},{... | collective-permute-start | bytes 884744 | tf_op jit(solution)/shard_map/ppermute | solution.py:33
  195.2 15.9 %collective-permute-done.25 = bf16[576,256]{1,0:T(8,128)(2,1)} collective-permute-done((bf16[576,256]{1,0:T(8,128)(2,1)}, bf16[576,256]{1,0:T(8,128)(2,1)}, u32[]{:S(2)}, u32[]{:S(2)}) %collective-permute-start.25) | collective-permute-done | bytes 294944 | tf_op jit(solution)/shard_map/ppermute | solution.py:33
  211.2 9.5 %collective-permute-start.29 = (bf16[576,256]{1,0:T(8,128)(2,1)}, bf16[576,256]{1,0:T(8,128)(2,1)S(1)}, u32[]{:S(2)}, u32[]{:S(2)}) collective-permute-start(bf16[576,256]{1,0:T(8,128)(2,1)} %get-tuple-element.86), channel_id=1, source_target_pairs={{0,28},{4,0},{8,4},{12,8},{16,12},{20,16},{24,20},{28,24},{1,29},{... | collective-permute-start | bytes 884744 | tf_op jit(solution)/shard_map/ppermute | solution.py:33
  220.7 8.8 %collective-permute-start.18 = (bf16[96,2048]{1,0:T(8,128)(2,1)S(1)}, bf16[96,2048]{1,0:T(8,128)(2,1)S(1)}, u32[]{:S(2)}, u32[]{:S(2)}) collective-permute-start(bf16[96,2048]{1,0:T(8,128)(2,1)S(1)} %copy-done.14), channel_id=1, source_target_pairs={{6,0},{7,1},{4,2},{5,3},{10,4},{11,5},{8,6},{9,7},{14,8},{15,9},{1... | collective-permute-start | bytes 1179656 | tf_op jit(solution)/shard_map/ppermute | solution.py:71
  234.9 6.4 %collective-permute-start.22 = (bf16[96,2048]{1,0:T(8,128)(2,1)S(1)}, bf16[96,2048]{1,0:T(8,128)(2,1)S(1)}, u32[]{:S(2)}, u32[]{:S(2)}) collective-permute-start(bf16[96,2048]{1,0:T(8,128)(2,1)S(1)} %copy-done.10), channel_id=1, source_target_pairs={{14,0},{15,1},{12,2},{13,3},{2,4},{3,5},{0,6},{1,7},{6,8},{7,9},{4... | collective-permute-start | bytes 1179656 | tf_op jit(solution)/shard_map/ppermute | solution.py:71
  243.0 8.4 %collective-permute-done.19 = bf16[96,2048]{1,0:T(8,128)(2,1)S(1)} collective-permute-done((bf16[96,2048]{1,0:T(8,128)(2,1)S(1)}, bf16[96,2048]{1,0:T(8,128)(2,1)S(1)}, u32[]{:S(2)}, u32[]{:S(2)}) %collective-permute-start.19) | collective-permute-done | bytes 393248 | tf_op jit(solution)/shard_map/ppermute | solution.py:71
  251.4 6.8 %collective-permute-done.20 = bf16[96,2048]{1,0:T(8,128)(2,1)S(1)} collective-permute-done((bf16[96,2048]{1,0:T(8,128)(2,1)S(1)}, bf16[96,2048]{1,0:T(8,128)(2,1)S(1)}, u32[]{:S(2)}, u32[]{:S(2)}) %collective-permute-start.20) | collective-permute-done | bytes 393248 | tf_op jit(solution)/shard_map/ppermute | solution.py:71
  258.2 7.0 %collective-permute-done.22 = bf16[96,2048]{1,0:T(8,128)(2,1)S(1)} collective-permute-done((bf16[96,2048]{1,0:T(8,128)(2,1)S(1)}, bf16[96,2048]{1,0:T(8,128)(2,1)S(1)}, u32[]{:S(2)}, u32[]{:S(2)}) %collective-permute-start.22) | collective-permute-done | bytes 393248 | tf_op jit(solution)/shard_map/ppermute | solution.py:71
  270.9 8.5 %collective-permute-done.30 = bf16[96,2048]{1,0:T(8,128)(2,1)S(1)} collective-permute-done((bf16[96,2048]{1,0:T(8,128)(2,1)S(1)}, bf16[96,2048]{1,0:T(8,128)(2,1)S(1)}, u32[]{:S(2)}, u32[]{:S(2)}) %collective-permute-start.30) | collective-permute-done | bytes 393248 | tf_op jit(solution)/shard_map/ppermute | solution.py:71
  279.4 6.6 %collective-permute-done.31 = bf16[96,2048]{1,0:T(8,128)(2,1)S(1)} collective-permute-done((bf16[96,2048]{1,0:T(8,128)(2,1)S(1)}, bf16[96,2048]{1,0:T(8,128)(2,1)S(1)}, u32[]{:S(2)}, u32[]{:S(2)}) %collective-permute-start.31) | collective-permute-done | bytes 393248 | tf_op jit(solution)/shard_map/ppermute | solution.py:71
  321.8 8.5 %collective-permute-done.35 = bf16[96,2048]{1,0:T(8,128)(2,1)S(1)} collective-permute-done((bf16[96,2048]{1,0:T(8,128)(2,1)S(1)}, bf16[96,2048]{1,0:T(8,128)(2,1)S(1)}, u32[]{:S(2)}, u32[]{:S(2)}) %collective-permute-start.35) | collective-permute-done | bytes 393248 | tf_op jit(solution)/shard_map/ppermute | solution.py:71
  330.3 8.6 %collective-permute-done.36 = bf16[96,2048]{1,0:T(8,128)(2,1)S(1)} collective-permute-done((bf16[96,2048]{1,0:T(8,128)(2,1)S(1)}, bf16[96,2048]{1,0:T(8,128)(2,1)S(1)}, u32[]{:S(2)}, u32[]{:S(2)}) %collective-permute-start.36) | collective-permute-done | bytes 393248 | tf_op jit(solution)/shard_map/ppermute | solution.py:71
  358.1 7.8 %collective-permute-done.40 = bf16[96,2048]{1,0:T(8,128)(2,1)S(1)} collective-permute-done((bf16[96,2048]{1,0:T(8,128)(2,1)}, bf16[96,2048]{1,0:T(8,128)(2,1)S(1)}, u32[]{:S(2)}, u32[]{:S(2)}) %collective-permute-start.40) | collective-permute-done | bytes 393248 | tf_op jit(solution)/shard_map/ppermute | solution.py:71
  366.7 11.5 %collective-permute-done.43 = bf16[96,2048]{1,0:T(8,128)(2,1)S(1)} collective-permute-done((bf16[96,2048]{1,0:T(8,128)(2,1)}, bf16[96,2048]{1,0:T(8,128)(2,1)S(1)}, u32[]{:S(2)}, u32[]{:S(2)}) %collective-permute-start.43) | collective-permute-done | bytes 393248 | tf_op jit(solution)/shard_map/ppermute | solution.py:71
  384.4 6.0 %collective-permute-start.47 = (bf16[1056,256]{1,0:T(8,128)(2,1)S(1)}, bf16[1056,256]{1,0:T(8,128)(2,1)S(1)}, u32[]{:S(2)}, u32[]{:S(2)}) collective-permute-start(bf16[1056,256]{1,0:T(8,128)(2,1)S(1)} %get-tuple-element.71), channel_id=1, source_target_pairs={{0,12},{4,16},{8,20},{12,24},{16,28},{20,0},{24,4},{28,8},{1,13},{... | collective-permute-start | bytes 1622024 | tf_op jit(solution)/shard_map/ppermute | solution.py:33
  391.7 12.1 %collective-permute-done.45 = bf16[1056,256]{1,0:T(8,128)(2,1)S(1)} collective-permute-done((bf16[1056,256]{1,0:T(8,128)(2,1)S(1)}, bf16[1056,256]{1,0:T(8,128)(2,1)S(1)}, u32[]{:S(2)}, u32[]{:S(2)}) %collective-permute-start.45) | collective-permute-done | bytes 540704 | tf_op jit(solution)/shard_map/ppermute | solution.py:33
  406.2 43.6 %collective-permute-done.47 = bf16[1056,256]{1,0:T(8,128)(2,1)S(1)} collective-permute-done((bf16[1056,256]{1,0:T(8,128)(2,1)S(1)}, bf16[1056,256]{1,0:T(8,128)(2,1)S(1)}, u32[]{:S(2)}, u32[]{:S(2)}) %collective-permute-start.47) | collective-permute-done | bytes 540704 | tf_op jit(solution)/shard_map/ppermute | solution.py:33
  449.9 12.9 %collective-permute-start.51 = (bf16[1056,256]{1,0:T(8,128)(2,1)S(1)}, bf16[1056,256]{1,0:T(8,128)(2,1)S(1)}, u32[]{:S(2)}, u32[]{:S(2)}) collective-permute-start(bf16[1056,256]{1,0:T(8,128)(2,1)S(1)} %get-tuple-element.67), channel_id=1, source_target_pairs={{0,28},{4,0},{8,4},{12,8},{16,12},{20,16},{24,20},{28,24},{1,29},{... | collective-permute-start | bytes 1622024 | tf_op jit(solution)/shard_map/ppermute | solution.py:33
  463.5 9.9 %collective-permute-done.51 = bf16[1056,256]{1,0:T(8,128)(2,1)S(1)} collective-permute-done((bf16[1056,256]{1,0:T(8,128)(2,1)S(1)}, bf16[1056,256]{1,0:T(8,128)(2,1)S(1)}, u32[]{:S(2)}, u32[]{:S(2)}) %collective-permute-start.51) | collective-permute-done | bytes 540704 | tf_op jit(solution)/shard_map/ppermute | solution.py:33
  487.0 13.1 %collective-permute-start.55 = (bf16[96,2048]{1,0:T(8,128)(2,1)S(1)}, bf16[96,2048]{1,0:T(8,128)(2,1)S(1)}, u32[]{:S(2)}, u32[]{:S(2)}) collective-permute-start(bf16[96,2048]{1,0:T(8,128)(2,1)S(1)} %get-tuple-element.59), channel_id=1, source_target_pairs={{4,0},{5,1},{6,2},{7,3},{8,4},{9,5},{10,6},{11,7},{12,8},{13,9},{1... | collective-permute-start | bytes 1179656 | tf_op jit(solution)/shard_map/ppermute | solution.py:71
  511.0 7.1 %collective-permute-done.56 = bf16[96,2048]{1,0:T(8,128)(2,1)S(1)} collective-permute-done((bf16[96,2048]{1,0:T(8,128)(2,1)S(1)}, bf16[96,2048]{1,0:T(8,128)(2,1)S(1)}, u32[]{:S(2)}, u32[]{:S(2)}) %collective-permute-start.56) | collective-permute-done | bytes 393248 | tf_op jit(solution)/shard_map/ppermute | solution.py:71
  518.1 8.4 %collective-permute-done.57 = bf16[96,2048]{1,0:T(8,128)(2,1)S(1)} collective-permute-done((bf16[96,2048]{1,0:T(8,128)(2,1)S(1)}, bf16[96,2048]{1,0:T(8,128)(2,1)S(1)}, u32[]{:S(2)}, u32[]{:S(2)}) %collective-permute-start.57) | collective-permute-done | bytes 393248 | tf_op jit(solution)/shard_map/ppermute | solution.py:71
  526.5 7.4 %collective-permute-done.58 = bf16[96,2048]{1,0:T(8,128)(2,1)S(1)} collective-permute-done((bf16[96,2048]{1,0:T(8,128)(2,1)S(1)}, bf16[96,2048]{1,0:T(8,128)(2,1)S(1)}, u32[]{:S(2)}, u32[]{:S(2)}) %collective-permute-start.58) | collective-permute-done | bytes 393248 | tf_op jit(solution)/shard_map/ppermute | solution.py:71
  (254 shorter events, 182.9 us)
Async XLA Ops:
  7.6 25.4 %collective-permute-start.2 = (bf16[96,2048]{1,0:T(8,128)(2,1)S(1)}, bf16[96,2048]{1,0:T(8,128)(2,1)S(1)}, u32[]{:S(2)}, u32[]{:S(2)}) collective-permute-start(bf16[96,2048]{1,0:T(8,128)(2,1)S(1)} %get-tuple-element.52), channel_id=1, source_target_pairs={{0,6},{1,7},{2,4},{3,5},{4,10},{5,11},{6,8},{7,9},{8,14},{9,15},{1... | collective-permute-start | bytes 1179656 | tf_op jit(solution)/shard_map/ppermute | solution.py:71
  9.1 24.7 %collective-permute-start.3 = (bf16[96,2048]{1,0:T(8,128)(2,1)S(1)}, bf16[96,2048]{1,0:T(8,128)(2,1)S(1)}, u32[]{:S(2)}, u32[]{:S(2)}) collective-permute-start(bf16[96,2048]{1,0:T(8,128)(2,1)S(1)} %get-tuple-element.52), channel_id=1, source_target_pairs={{0,8},{1,9},{2,10},{3,11},{4,12},{5,13},{6,14},{7,15},{8,0},{9,1},... | collective-permute-start | bytes 1179656 | tf_op jit(solution)/shard_map/ppermute | solution.py:71
  9.2 25.4 %collective-permute-start.4 = (bf16[96,2048]{1,0:T(8,128)(2,1)S(1)}, bf16[96,2048]{1,0:T(8,128)(2,1)S(1)}, u32[]{:S(2)}, u32[]{:S(2)}) collective-permute-start(bf16[96,2048]{1,0:T(8,128)(2,1)S(1)} %get-tuple-element.52), channel_id=1, source_target_pairs={{0,10},{1,11},{2,8},{3,9},{4,14},{5,15},{6,12},{7,13},{8,2},{9,3},... | collective-permute-start | bytes 1179656 | tf_op jit(solution)/shard_map/ppermute | solution.py:71
  16.1 26.9 %collective-permute-start.5 = (bf16[96,2048]{1,0:T(8,128)(2,1)S(1)}, bf16[96,2048]{1,0:T(8,128)(2,1)S(1)}, u32[]{:S(2)}, u32[]{:S(2)}) collective-permute-start(bf16[96,2048]{1,0:T(8,128)(2,1)S(1)} %get-tuple-element.52), channel_id=1, source_target_pairs={{0,12},{1,13},{2,14},{3,15},{4,0},{5,1},{6,2},{7,3},{8,4},{9,5},{1... | collective-permute-start | bytes 1179656 | tf_op jit(solution)/shard_map/ppermute | solution.py:71
  19.9 26.5 %collective-permute-start.6 = (bf16[96,2048]{1,0:T(8,128)(2,1)S(1)}, bf16[96,2048]{1,0:T(8,128)(2,1)S(1)}, u32[]{:S(2)}, u32[]{:S(2)}) collective-permute-start(bf16[96,2048]{1,0:T(8,128)(2,1)S(1)} %get-tuple-element.52), channel_id=1, source_target_pairs={{0,14},{1,15},{2,12},{3,13},{4,2},{5,3},{6,0},{7,1},{8,6},{9,7},{1... | collective-permute-start | bytes 1179656 | tf_op jit(solution)/shard_map/ppermute | solution.py:71
  47.2 92.7 %collective-permute-start.14 = (bf16[768,2048]{1,0:T(8,128)(2,1)}, bf16[768,2048]{1,0:T(8,128)(2,1)}, u32[]{:S(2)}, u32[]{:S(2)}) collective-permute-start(bf16[768,2048]{1,0:T(8,128)(2,1)} %constant_dynamic-update-slice_fusion), channel_id=1, source_target_pairs={{0,1},{1,0},{2,3},{3,2},{4,5},{5,4},{6,7},{7,6},{8,9},{9,8},{10,11... | collective-permute-start | bytes 9437192 | tf_op jit(solution)/shard_map/ppermute | solution.py:67
  56.4 61.0 %collective-permute-start.9 = (bf16[1056,256]{1,0:T(8,128)(2,1)}, bf16[1056,256]{1,0:T(8,128)(2,1)}, u32[]{:S(2)}, u32[]{:S(2)}) collective-permute-start(bf16[1056,256]{1,0:T(8,128)(2,1)} %get-tuple-element.78), channel_id=1, source_target_pairs={{0,12},{4,16},{8,20},{12,24},{16,28},{20,0},{24,4},{28,8},{1,13},{... | collective-permute-start | bytes 1622024 | tf_op jit(solution)/shard_map/ppermute | solution.py:33
  57.5 76.5 %collective-permute-start.10 = (bf16[1056,256]{1,0:T(8,128)(2,1)}, bf16[1056,256]{1,0:T(8,128)(2,1)}, u32[]{:S(2)}, u32[]{:S(2)}) collective-permute-start(bf16[1056,256]{1,0:T(8,128)(2,1)} %get-tuple-element.77), channel_id=1, source_target_pairs={{0,16},{4,20},{8,24},{12,28},{16,0},{20,4},{24,8},{28,12},{1,17},{... | collective-permute-start | bytes 1622024 | tf_op jit(solution)/shard_map/ppermute | solution.py:33
  71.2 64.8 %collective-permute-start.11 = (bf16[1056,256]{1,0:T(8,128)(2,1)}, bf16[1056,256]{1,0:T(8,128)(2,1)S(1)}, u32[]{:S(2)}, u32[]{:S(2)}) collective-permute-start(bf16[1056,256]{1,0:T(8,128)(2,1)} %get-tuple-element.76), channel_id=1, source_target_pairs={{0,20},{4,24},{8,28},{12,0},{16,4},{20,8},{24,12},{28,16},{1,21},{... | collective-permute-start | bytes 1622024 | tf_op jit(solution)/shard_map/ppermute | solution.py:33
  73.9 63.0 %collective-permute-start.12 = (bf16[1056,256]{1,0:T(8,128)(2,1)S(1)}, bf16[1056,256]{1,0:T(8,128)(2,1)S(1)}, u32[]{:S(2)}, u32[]{:S(2)}) collective-permute-start(bf16[1056,256]{1,0:T(8,128)(2,1)S(1)} %get-tuple-element.75), channel_id=1, source_target_pairs={{0,24},{4,28},{8,0},{12,4},{16,8},{20,12},{24,16},{28,20},{1,25},{... | collective-permute-start | bytes 1622024 | tf_op jit(solution)/shard_map/ppermute | solution.py:33
  151.7 33.8 %collective-permute-start.23 = (bf16[576,256]{1,0:T(8,128)(2,1)S(1)}, bf16[576,256]{1,0:T(8,128)(2,1)S(1)}, u32[]{:S(2)}, u32[]{:S(2)}) collective-permute-start(bf16[576,256]{1,0:T(8,128)(2,1)S(1)} %get-tuple-element.92), channel_id=1, source_target_pairs={{0,4},{4,8},{8,12},{12,16},{16,20},{20,24},{24,28},{28,0},{1,5},{5... | collective-permute-start | bytes 884744 | tf_op jit(solution)/shard_map/ppermute | solution.py:33
  166.4 27.9 %collective-permute-start.24 = (bf16[576,256]{1,0:T(8,128)(2,1)}, bf16[576,256]{1,0:T(8,128)(2,1)}, u32[]{:S(2)}, u32[]{:S(2)}) collective-permute-start(bf16[576,256]{1,0:T(8,128)(2,1)} %get-tuple-element.91), channel_id=1, source_target_pairs={{0,8},{4,12},{8,16},{12,20},{16,24},{20,28},{24,0},{28,4},{1,9},{5... | collective-permute-start | bytes 884744 | tf_op jit(solution)/shard_map/ppermute | solution.py:33
  181.6 29.5 %collective-permute-start.25 = (bf16[576,256]{1,0:T(8,128)(2,1)}, bf16[576,256]{1,0:T(8,128)(2,1)}, u32[]{:S(2)}, u32[]{:S(2)}) collective-permute-start(bf16[576,256]{1,0:T(8,128)(2,1)} %get-tuple-element.90), channel_id=1, source_target_pairs={{0,12},{4,16},{8,20},{12,24},{16,28},{20,0},{24,4},{28,8},{1,13},{... | collective-permute-start | bytes 884744 | tf_op jit(solution)/shard_map/ppermute | solution.py:33
  184.3 36.4 %collective-permute-start.26 = (bf16[576,256]{1,0:T(8,128)(2,1)}, bf16[576,256]{1,0:T(8,128)(2,1)}, u32[]{:S(2)}, u32[]{:S(2)}) collective-permute-start(bf16[576,256]{1,0:T(8,128)(2,1)} %get-tuple-element.89), channel_id=1, source_target_pairs={{0,16},{4,20},{8,24},{12,28},{16,0},{20,4},{24,8},{28,12},{1,17},{... | collective-permute-start | bytes 884744 | tf_op jit(solution)/shard_map/ppermute | solution.py:33
  186.3 48.5 %collective-permute-start.17 = (bf16[96,2048]{1,0:T(8,128)(2,1)}, bf16[96,2048]{1,0:T(8,128)(2,1)S(1)}, u32[]{:S(2)}, u32[]{:S(2)}) collective-permute-start(bf16[96,2048]{1,0:T(8,128)(2,1)} %get-tuple-element.66), channel_id=1, source_target_pairs={{4,0},{5,1},{6,2},{7,3},{8,4},{9,5},{10,6},{11,7},{12,8},{13,9},{1... | collective-permute-start | bytes 1179656 | tf_op jit(solution)/shard_map/ppermute | solution.py:71
  188.1 43.4 %collective-permute-start.27 = (bf16[576,256]{1,0:T(8,128)(2,1)}, bf16[576,256]{1,0:T(8,128)(2,1)S(1)}, u32[]{:S(2)}, u32[]{:S(2)}) collective-permute-start(bf16[576,256]{1,0:T(8,128)(2,1)} %get-tuple-element.88), channel_id=1, source_target_pairs={{0,20},{4,24},{8,28},{12,0},{16,4},{20,8},{24,12},{28,16},{1,21},{... | collective-permute-start | bytes 884744 | tf_op jit(solution)/shard_map/ppermute | solution.py:33
  194.3 39.9 %collective-permute-start.28 = (bf16[576,256]{1,0:T(8,128)(2,1)}, bf16[576,256]{1,0:T(8,128)(2,1)S(1)}, u32[]{:S(2)}, u32[]{:S(2)}) collective-permute-start(bf16[576,256]{1,0:T(8,128)(2,1)} %get-tuple-element.87), channel_id=1, source_target_pairs={{0,24},{4,28},{8,0},{12,4},{16,8},{20,12},{24,16},{28,20},{1,25},{... | collective-permute-start | bytes 884744 | tf_op jit(solution)/shard_map/ppermute | solution.py:33
  211.2 23.7 %collective-permute-start.29 = (bf16[576,256]{1,0:T(8,128)(2,1)}, bf16[576,256]{1,0:T(8,128)(2,1)S(1)}, u32[]{:S(2)}, u32[]{:S(2)}) collective-permute-start(bf16[576,256]{1,0:T(8,128)(2,1)} %get-tuple-element.86), channel_id=1, source_target_pairs={{0,28},{4,0},{8,4},{12,8},{16,12},{20,16},{24,20},{28,24},{1,29},{... | collective-permute-start | bytes 884744 | tf_op jit(solution)/shard_map/ppermute | solution.py:33
  234.2 24.0 %collective-permute-start.20 = (bf16[96,2048]{1,0:T(8,128)(2,1)S(1)}, bf16[96,2048]{1,0:T(8,128)(2,1)S(1)}, u32[]{:S(2)}, u32[]{:S(2)}) collective-permute-start(bf16[96,2048]{1,0:T(8,128)(2,1)S(1)} %copy-done.12), channel_id=1, source_target_pairs={{10,0},{11,1},{8,2},{9,3},{14,4},{15,5},{12,6},{13,7},{2,8},{3,9},... | collective-permute-start | bytes 1179656 | tf_op jit(solution)/shard_map/ppermute | solution.py:71
  234.9 30.4 %collective-permute-start.22 = (bf16[96,2048]{1,0:T(8,128)(2,1)S(1)}, bf16[96,2048]{1,0:T(8,128)(2,1)S(1)}, u32[]{:S(2)}, u32[]{:S(2)}) collective-permute-start(bf16[96,2048]{1,0:T(8,128)(2,1)S(1)} %copy-done.10), channel_id=1, source_target_pairs={{14,0},{15,1},{12,2},{13,3},{2,4},{3,5},{0,6},{1,7},{6,8},{7,9},{4... | collective-permute-start | bytes 1179656 | tf_op jit(solution)/shard_map/ppermute | solution.py:71
  353.1 25.2 %collective-permute-start.43 = (bf16[96,2048]{1,0:T(8,128)(2,1)}, bf16[96,2048]{1,0:T(8,128)(2,1)S(1)}, u32[]{:S(2)}, u32[]{:S(2)}) collective-permute-start(bf16[96,2048]{1,0:T(8,128)(2,1)} %get-tuple-element.46), channel_id=1, source_target_pairs={{0,12},{1,13},{2,14},{3,15},{4,0},{5,1},{6,2},{7,3},{8,4},{9,5},{1... | collective-permute-start | bytes 1179656 | tf_op jit(solution)/shard_map/ppermute | solution.py:71
  355.2 24.6 %collective-permute-start.44 = (bf16[96,2048]{1,0:T(8,128)(2,1)}, bf16[96,2048]{1,0:T(8,128)(2,1)S(1)}, u32[]{:S(2)}, u32[]{:S(2)}) collective-permute-start(bf16[96,2048]{1,0:T(8,128)(2,1)} %get-tuple-element.46), channel_id=1, source_target_pairs={{0,14},{1,15},{2,12},{3,13},{4,2},{5,3},{6,0},{7,1},{8,6},{9,7},{1... | collective-permute-start | bytes 1179656 | tf_op jit(solution)/shard_map/ppermute | solution.py:71
  379.8 94.1 %collective-permute-start.52 = (bf16[768,2048]{1,0:T(8,128)(2,1)S(1)}, bf16[768,2048]{1,0:T(8,128)(2,1)S(1)}, u32[]{:S(2)}, u32[]{:S(2)}) collective-permute-start(bf16[768,2048]{1,0:T(8,128)(2,1)S(1)} %constant_dynamic-update-slice_fusion.8), channel_id=1, source_target_pairs={{0,1},{1,0},{2,3},{3,2},{4,5},{5,4},{6,7},{7,6},{8,9},{9,8},{10,11... | collective-permute-start | bytes 9437192 | tf_op jit(solution)/shard_map/ppermute | solution.py:67
  380.1 23.6 %collective-permute-start.45 = (bf16[1056,256]{1,0:T(8,128)(2,1)S(1)}, bf16[1056,256]{1,0:T(8,128)(2,1)S(1)}, u32[]{:S(2)}, u32[]{:S(2)}) collective-permute-start(bf16[1056,256]{1,0:T(8,128)(2,1)S(1)} %get-tuple-element.73), channel_id=1, source_target_pairs={{0,4},{4,8},{8,12},{12,16},{16,20},{20,24},{24,28},{28,0},{1,5},{5... | collective-permute-start | bytes 1622024 | tf_op jit(solution)/shard_map/ppermute | solution.py:33
  384.4 65.4 %collective-permute-start.47 = (bf16[1056,256]{1,0:T(8,128)(2,1)S(1)}, bf16[1056,256]{1,0:T(8,128)(2,1)S(1)}, u32[]{:S(2)}, u32[]{:S(2)}) collective-permute-start(bf16[1056,256]{1,0:T(8,128)(2,1)S(1)} %get-tuple-element.71), channel_id=1, source_target_pairs={{0,12},{4,16},{8,20},{12,24},{16,28},{20,0},{24,4},{28,8},{1,13},{... | collective-permute-start | bytes 1622024 | tf_op jit(solution)/shard_map/ppermute | solution.py:33
  390.4 73.0 %collective-permute-start.48 = (bf16[1056,256]{1,0:T(8,128)(2,1)S(1)}, bf16[1056,256]{1,0:T(8,128)(2,1)S(1)}, u32[]{:S(2)}, u32[]{:S(2)}) collective-permute-start(bf16[1056,256]{1,0:T(8,128)(2,1)S(1)} %get-tuple-element.70), channel_id=1, source_target_pairs={{0,16},{4,20},{8,24},{12,28},{16,0},{20,4},{24,8},{28,12},{1,17},{... | collective-permute-start | bytes 1622024 | tf_op jit(solution)/shard_map/ppermute | solution.py:33
  403.8 59.7 %collective-permute-start.49 = (bf16[1056,256]{1,0:T(8,128)(2,1)S(1)}, bf16[1056,256]{1,0:T(8,128)(2,1)S(1)}, u32[]{:S(2)}, u32[]{:S(2)}) collective-permute-start(bf16[1056,256]{1,0:T(8,128)(2,1)S(1)} %get-tuple-element.69), channel_id=1, source_target_pairs={{0,20},{4,24},{8,28},{12,0},{16,4},{20,8},{24,12},{28,16},{1,21},{... | collective-permute-start | bytes 1622024 | tf_op jit(solution)/shard_map/ppermute | solution.py:33
  404.4 59.0 %collective-permute-start.50 = (bf16[1056,256]{1,0:T(8,128)(2,1)S(1)}, bf16[1056,256]{1,0:T(8,128)(2,1)S(1)}, u32[]{:S(2)}, u32[]{:S(2)}) collective-permute-start(bf16[1056,256]{1,0:T(8,128)(2,1)S(1)} %get-tuple-element.68), channel_id=1, source_target_pairs={{0,24},{4,28},{8,0},{12,4},{16,8},{20,12},{24,16},{28,20},{1,25},{... | collective-permute-start | bytes 1622024 | tf_op jit(solution)/shard_map/ppermute | solution.py:33
  500.9 25.7 %collective-permute-start.57 = (bf16[96,2048]{1,0:T(8,128)(2,1)S(1)}, bf16[96,2048]{1,0:T(8,128)(2,1)S(1)}, u32[]{:S(2)}, u32[]{:S(2)}) collective-permute-start(bf16[96,2048]{1,0:T(8,128)(2,1)S(1)} %get-tuple-element.57), channel_id=1, source_target_pairs={{8,0},{9,1},{10,2},{11,3},{12,4},{13,5},{14,6},{15,7},{0,8},{1,9},... | collective-permute-start | bytes 1179656 | tf_op jit(solution)/shard_map/ppermute | solution.py:71
  500.9 33.0 %collective-permute-start.58 = (bf16[96,2048]{1,0:T(8,128)(2,1)S(1)}, bf16[96,2048]{1,0:T(8,128)(2,1)S(1)}, u32[]{:S(2)}, u32[]{:S(2)}) collective-permute-start(bf16[96,2048]{1,0:T(8,128)(2,1)S(1)} %get-tuple-element.56), channel_id=1, source_target_pairs={{10,0},{11,1},{8,2},{9,3},{14,4},{15,5},{12,6},{13,7},{2,8},{3,9},... | collective-permute-start | bytes 1179656 | tf_op jit(solution)/shard_map/ppermute | solution.py:71
  503.4 30.6 %collective-permute-start.59 = (bf16[96,2048]{1,0:T(8,128)(2,1)S(1)}, bf16[96,2048]{1,0:T(8,128)(2,1)S(1)}, u32[]{:S(2)}, u32[]{:S(2)}) collective-permute-start(bf16[96,2048]{1,0:T(8,128)(2,1)S(1)} %get-tuple-element.55), channel_id=1, source_target_pairs={{12,0},{13,1},{14,2},{15,3},{0,4},{1,5},{2,6},{3,7},{4,8},{5,9},{6... | collective-permute-start | bytes 1179656 | tf_op jit(solution)/shard_map/ppermute | solution.py:71
  509.6 28.5 %collective-permute-start.60 = (bf16[96,2048]{1,0:T(8,128)(2,1)S(1)}, bf16[96,2048]{1,0:T(8,128)(2,1)S(1)}, u32[]{:S(2)}, u32[]{:S(2)}) collective-permute-start(bf16[96,2048]{1,0:T(8,128)(2,1)S(1)} %get-tuple-element.54), channel_id=1, source_target_pairs={{14,0},{15,1},{12,2},{13,3},{2,4},{3,5},{0,6},{1,7},{6,8},{7,9},{4... | collective-permute-start | bytes 1179656 | tf_op jit(solution)/shard_map/ppermute | solution.py:71
  (57 other events, 1067.4 us)
